TPU v7x, 32 devices: a whole 2x2x4 slice. The times are simulated.
32 devices in a mesh: vp: 8 (over z, x), dp: 4 (over y, core).
Axes of the slice: x: 2, y: 2, z: 4, core: 2. Of those that a mesh axis runs over, the one named last changes fastest.
Arguments:
- stream: bfloat16 [1024, 2048], P(('dp', 'vp')), may hold values from -60 to 60
- hidden: bfloat16 [1024, 5632], P('dp', 'vp'), may hold values from -6 to 6
- w_down: bfloat16 [5632, 2048], P(None, 'vp'), may hold values from -0.078125 to 0.078125
- final_gain: float32 [2048], replicated, may hold values from 0.1 to 1.9
- vocab: bfloat16 [2048, 32768], P(None, 'vp'), may hold values from -2 to 200
- vocab_bias: float32 [32768], P('vp'), may hold values from -5 to 5
- targets: int32 [1024], P('dp'), may hold values from 0 to 32767
Outputs:
- losses: float32 [1024], P(('dp', 'vp'))
- grad_input: float32 [1024, 2048], P(('dp', 'vp'))
- grad_vocab: float32 [2048, 32768], P('dp', 'vp')
All inputs are finite; a program needn't handle non-finite values.
Results may differ from a plain program's by a relative error of at most 0.02.
Values may be sent and summed in bfloat16 or wider, within the bound.
A program may use at most 128 MiB of HBM per device.

v0:
```python
import jax
import jax.numpy as jnp
from jax import lax
from jax.sharding import PartitionSpec as P

norm_eps = 1e-06
zloss_weight = 0.001


def combined_all(value, axis, join):
    pieces = jax.tree.map(lambda part: lax.all_gather(part, axis), value)
    head = jax.tree.map(lambda part: part[0], pieces)
    tail = jax.tree.map(lambda part: part[1:], pieces)
    total, _ = lax.scan(lambda total, section: (join(total, section), None), head, tail)
    return total


def combine_stats(first, second):
    top = jnp.maximum(first[0], second[0])
    total = first[1] * jnp.exp(first[0] - top) + second[1] * jnp.exp(second[0] - top)
    return (top, total, first[2] + second[2])


def body(stream, hidden, w_down, final_gain, vocab, vocab_bias, targets):
    rows_dev = stream.shape[0]
    width = stream.shape[1]
    group = targets.shape[0]
    mine = lax.axis_index("vp")
    feat_cols = w_down.shape[1]
    proj = jnp.dot(
        lax.all_gather(hidden, "vp", axis=1, tiled=True), w_down, preferred_element_type=jnp.float32
    )
    stream_cols = lax.all_to_all(stream, "vp", split_axis=1, concat_axis=0, tiled=True)
    normin_cols = (stream_cols.astype(jnp.float32) + proj).astype(jnp.bfloat16)
    col_values = normin_cols.astype(jnp.float32)
    square_total = lax.psum(jnp.sum(col_values * col_values, axis=1), "vp")
    inv_group = lax.rsqrt(square_total / width + norm_eps)
    gain_cols = lax.dynamic_slice_in_dim(final_gain, mine * feat_cols, feat_cols)
    normed_cols = (col_values * inv_group[:, None] * gain_cols).astype(jnp.bfloat16)
    normed = lax.all_gather(normed_cols, "vp", axis=1, tiled=True)
    normin = lax.all_to_all(normin_cols, "vp", split_axis=0, concat_axis=1, tiled=True)
    values = normin.astype(jnp.float32)
    inv = lax.rsqrt(jnp.mean(values * values, axis=1, keepdims=True) + norm_eps)
    ncols = vocab.shape[1]
    scores = jnp.dot(normed, vocab, preferred_element_type=jnp.float32) + vocab_bias
    local_top = jnp.max(scores, axis=1)
    local_total = jnp.sum(jnp.exp(scores - local_top[:, None]), axis=1)
    column_ids = lax.broadcasted_iota(jnp.int32, (group, ncols), 1) + mine * ncols
    hit = column_ids == targets[:, None]
    local_target = jnp.sum(jnp.where(hit, scores, 0.0), axis=1)
    top, total, target_score = combined_all(
        (local_top, local_total, local_target), "vp", combine_stats
    )
    lse = top + jnp.log(total)
    group_losses = lse - target_score + zloss_weight * lse * lse
    losses = lax.dynamic_slice_in_dim(group_losses, mine * rows_dev, rows_dev)
    probs = jnp.exp(scores - lse[:, None])
    dscore = (probs * (1.0 + 2.0 * zloss_weight * lse)[:, None] - jnp.where(hit, 1.0, 0.0)).astype(
        jnp.bfloat16
    )
    feat_group = width // lax.axis_size("dp")
    feat_start = lax.axis_index("dp") * feat_group
    rows_slice = lax.dynamic_slice_in_dim(
        lax.all_gather(normed, "dp", axis=0, tiled=True), feat_start, feat_group, 1
    )
    grad_vocab = lax.dot_general(
        rows_slice,
        lax.all_gather(dscore, "dp", axis=0, tiled=True),
        (((0,), (0,)), ((), ())),
        preferred_element_type=jnp.float32,
    )
    row_term = lax.dot_general(
        dscore, vocab, (((1,), (1,)), ((), ())), preferred_element_type=jnp.float32
    )
    row_parts = lax.all_to_all(
        row_term[:, None, :].astype(jnp.bfloat16), "vp", split_axis=0, concat_axis=1, tiled=True
    ).astype(jnp.float32)
    dnormed = jnp.sum(row_parts, axis=1)
    scaled = dnormed * final_gain
    grad_input = inv * (
        scaled - values * inv * inv * jnp.mean(values * scaled, axis=1, keepdims=True)
    )
    return (losses, grad_input, grad_vocab)


def solution(mesh):
    placed = (
        P(("dp", "vp"), None),
        P("dp", "vp"),
        P(None, "vp"),
        P(),
        P(None, "vp"),
        P("vp"),
        P("dp"),
    )
    return jax.shard_map(
        body,
        mesh=mesh,
        in_specs=placed,
        out_specs=(P(("dp", "vp")), P(("dp", "vp"), None), P("dp", "vp")),
        check_vma=False,
    )
```

profile of v0, /device:TPU:0, one launch (start us, length us, event | category | flops | bytes accessed | tf_op | source)
XLA Modules:
  0.0 277.1 jit_solution(3364702741128540911)
XLA Ops:
  7.9 1.7 copy.29
  9.6 7.3 %all-to-all-start = ((bf16[32,8,256]{2,0,1:T(8,128)(2,1)}), bf16[32,8,256]{2,0,1:T(8,128)(2,1)S(1)}, u32[]{:S(2)}, u32[]{:S(2)}) async-start(bf16[32,8,256]{2,0,1:T(8,128)(2,1)} %bitcast.50), calls=%async_computation | async-start | bytes 262144 | tf_op jit(solution)/shard_map/all_to_all | solution.py:33
  17.7 6.6 %all-to-all-done = bf16[32,8,256]{2,0,1:T(8,128)(2,1)S(1)} async-done(((bf16[32,8,256]{2,0,1:T(8,128)(2,1)}), bf16[32,8,256]{2,0,1:T(8,128)(2,1)S(1)}, u32[]{:S(2)}, u32[]{:S(2)}) %all-to-all-start) | async-done | bytes 131104 | tf_op jit(solution)/shard_map/all_to_all | solution.py:33
  24.4 45.9 %all-gather.11.cloned.1.call-done = bf16[256,5632]{0,1:T(8,128)(2,1)} async-done(((bf16[256,704]{0,1:T(8,128)(2,1)}), bf16[256,5632]{0,1:T(8,128)(2,1)}) %all-gather.11.cloned.1.call-update) | async-done | bytes 2883600 | tf_op jit(solution)/shard_map/all_gather | solution.py:31
  70.2 3.4 %fusion.9 = (f32[256]{0:T(256)S(1)}, bf16[256,256]{1,0:T(8,128)(2,1)}) fusion(f32[256,256]{1,0:T(8,128)S(1)} %bitcast.63, bf16[256,5632]{0,1:T(8,128)(2,1)} %all-gather.11.cloned.1.call-done, bf16[5632,256]{1,0:T(8,128)(2,1)S(1)} %copy-done), kind=kOutput, calls=%fused_computation.23 | convolution fusion | flops 738524928 | bytes 6161408 | tf_op jit(solution)/shard_map/dot_general | solution.py:30
  73.7 19.0 %psum.7 = f32[256]{0:T(256)S(1)} all-reduce(f32[256]{0:T(256)S(1)} %get-tuple-element.69), channel_id=1, replica_groups=mesh['vp'=8,'dp'=4] {'vp'}, use_global_device_ids=true, to_apply=%region_1.0 | all-reduce | flops 256 | bytes 2048 | tf_op jit(solution)/shard_map/psum | solution.py:36
  92.7 1.7 fusion.11
  94.5 36.7 %all-gather.13.cloned.1.call-done = bf16[256,2048]{1,0:T(8,128)(2,1)} async-done(((bf16[256,256]{1,0:T(8,128)(2,1)}), bf16[256,2048]{1,0:T(8,128)(2,1)}) %all-gather.13.cloned.1.call-update) | async-done | bytes 1048592 | tf_op jit(solution)/shard_map/all_gather | solution.py:40
  131.3 8.5 %fusion.16 = (f32[256]{0:T(256)S(1)}, f32[256,4096]{1,0:T(8,128)S(1)}) fusion(f32[4096]{0:T(1024)S(1)} %copy-done.4, bf16[256,2048]{1,0:T(8,128)(2,1)} %all-gather.13.cloned.1.call-done, bf16[2048,4096]{1,0:T(8,128)(2,1)} %param.13), kind=kOutput, calls=%fused_computation.43 | convolution fusion | flops 4297064448 | bytes 22037504 | tf_op jit(solution)/shard_map/dot_general | solution.py:45
  139.9 18.4 %all-gather.3 = f32[8,1,256]{2,1,0:T(1,128)S(1)} all-gather(f32[1,1,256]{2,1,0:T(1,128)S(1)} %bitcast.74), channel_id=2, replica_groups=mesh['vp'=8,'dp'=4] {'vp'}, dimensions={0}, use_global_device_ids=true | all-gather | bytes 9216 | tf_op jit(solution)/shard_map/all_gather | solution.py:11
  158.3 1.3 fusion
  159.6 16.3 %all-gather.4 = f32[8,1,256]{2,1,0:T(1,128)S(1)} all-gather(f32[1,1,256]{2,1,0:T(1,128)S(1)} %bitcast.76), channel_id=3, replica_groups=mesh['vp'=8,'dp'=4] {'vp'}, dimensions={0}, use_global_device_ids=true | all-gather | bytes 9216 | tf_op jit(solution)/shard_map/all_gather | solution.py:11
  175.9 18.3 %all-gather.5 = f32[8,1,256]{2,1,0:T(1,128)S(1)} all-gather(f32[1,1,256]{2,1,0:T(1,128)S(1)} %bitcast.75), channel_id=4, replica_groups=mesh['vp'=8,'dp'=4] {'vp'}, dimensions={0}, use_global_device_ids=true | all-gather | bytes 9216 | tf_op jit(solution)/shard_map/all_gather | solution.py:11
  194.8 4.9 %fusion.2 = bf16[256,4096]{1,0:T(8,128)(2,1)} fusion(f32[256,4096]{1,0:T(8,128)} %copy-done.1, f32[256]{0:T(256)S(1)} %get-tuple-element.65, f32[256]{0:T(256)S(1)} %get-tuple-element.66, s32[4096]{0:T(1024)S(1)} %iota_add_fusion, s32[256]{0:T(256)S(1)} %copy-done.3), kind=kLoop, calls=%fused_computation.9 | loop fusion | flops 6291456 | bytes 6310912 | tf_op jit(solution)/shard_map/convert_element_type | solution.py:58
  199.7 3.4 %all-to-all-start.1 = ((bf16[8,32,256]{2,1,0:T(8,128)(2,1)}), bf16[8,32,256]{2,1,0:T(8,128)(2,1)S(1)}, u32[]{:S(2)}, u32[]{:S(2)}) async-start(bf16[8,32,256]{2,1,0:T(8,128)(2,1)} %bitcast.11), calls=%async_computation.1 | async-start | bytes 262144 | tf_op jit(solution)/shard_map/all_to_all | solution.py:41
  203.1 14.3 %fusion.3 = bf16[256,1,2048]{2,0,1:T(8,128)(2,1)} fusion(bf16[256,4096]{1,0:T(8,128)(2,1)} %fusion.2, bf16[2048,4096]{1,0:T(8,128)(2,1)} %param.13), kind=kOutput, calls=%fused_computation.12 | convolution fusion | flops 4295491584 | bytes 19922944 | tf_op jit(solution)/shard_map/dot_general | solution.py:72
  218.0 3.4 %reduce.5 = bf16[256,2048]{1,0:T(8,128)(2,1)} reduce(bf16[256,1,2048]{2,0,1:T(8,128)(2,1)} %fusion.3, bf16[]{:T(256)} %broadcast.36), dimensions={1}, to_apply=%copy.14.reduce_sub_computation | reduce | bytes 2097154 | tf_op jit(solution)/shard_map/convert_element_type | solution.py:76
  221.3 2.6 reshape.76
  223.9 6.1 %all-to-all-start.2 = ((bf16[8,2,32768]{2,1,0:T(2,128)(2,1)}), bf16[8,2,32768]{2,1,0:T(2,128)(2,1)}, u32[]{:S(2)}, u32[]{:S(2)}) async-start(bf16[8,2,32768]{2,1,0:T(2,128)(2,1)} %reshape.76), calls=%async_computation.2 | async-start | bytes 2097152 | tf_op jit(solution)/shard_map/all_to_all | solution.py:75
  230.7 15.8 %all-to-all-done.2 = bf16[8,2,32768]{2,1,0:T(2,128)(2,1)} async-done(((bf16[8,2,32768]{2,1,0:T(2,128)(2,1)}), bf16[8,2,32768]{2,1,0:T(2,128)(2,1)}, u32[]{:S(2)}, u32[]{:S(2)}) %all-to-all-start.2) | async-done | bytes 1048608 | tf_op jit(solution)/shard_map/all_to_all | solution.py:75
  246.5 5.8 %reshape.77 = bf16[256,1,2048]{2,1,0:T(2,128)(2,1)} reshape(bf16[8,2,32768]{2,1,0:T(2,128)(2,1)} %all-to-all-done.2) | data formatting | bytes 2097152
  252.3 3.8 %copy.20 = f32[256,1,2048]{2,0,1:T(8,128)} copy(bf16[256,1,2048]{2,1,0:T(2,128)(2,1)} %reshape.77) | data formatting | bytes 3145728
  256.1 1.7 reduce_sum.60
  258.9 11.7 %fusion.5 = f32[512,4096]{1,0:T(8,128)} fusion(bf16[1024,4096]{1,0:T(8,128)(2,1)} %all-gather.17.cloned.1.call-done, bf16[1024,2048]{1,0:T(8,128)(2,1)} %all-gather.15.cloned.1.call-done, s32[]{:T(128)S(6)} %select_n.21), kind=kOutput, calls=%fused_computation.15 | convolution fusion | flops 4294967296 | bytes 17825796 | tf_op jit(solution)/shard_map/dot_general | solution.py:66
  (73 shorter events, 4.8 us)
Async XLA Ops:
  7.2 63.1 %copy-start = (bf16[5632,256]{1,0:T(8,128)(2,1)S(1)}, bf16[5632,256]{1,0:T(8,128)(2,1)}, u32[]{:S(2)}) copy-start(bf16[5632,256]{1,0:T(8,128)(2,1)} %param.11) | copy-start | bytes 8650756
  7.2 63.0 %all-gather.11.cloned.1.call-start = ((), (), s32[]{:S(2)}) async-start(), calls=%async_computation.3 | async-start | bytes 3244032 | tf_op jit(solution)/shard_map/all_gather | solution.py:31
  9.6 14.7 %all-to-all-start = ((bf16[32,8,256]{2,0,1:T(8,128)(2,1)}), bf16[32,8,256]{2,0,1:T(8,128)(2,1)S(1)}, u32[]{:S(2)}, u32[]{:S(2)}) async-start(bf16[32,8,256]{2,0,1:T(8,128)(2,1)} %bitcast.50), calls=%async_computation | async-start | bytes 262144 | tf_op jit(solution)/shard_map/all_to_all | solution.py:33
  16.9 114.3 %all-gather.13.cloned.1.call-start = ((), (), s32[]{:S(2)}) async-start(), calls=%async_computation.4 | async-start | bytes 1179648 | tf_op jit(solution)/shard_map/all_gather | solution.py:40
  70.2 61.1 %copy-start.4 = (f32[4096]{0:T(1024)S(1)}, f32[4096]{0:T(1024)}, u32[]{:S(2)}) copy-start(f32[4096]{0:T(1024)} %param.14) | copy-start | bytes 49156
  94.4 164.4 %all-gather.15.cloned.1.call-start = ((), (), s32[]{:S(2)}) async-start(), calls=%async_computation.5 | async-start | bytes 5242880 | tf_op jit(solution)/shard_map/all_gather | solution.py:64
  131.2 127.6 %all-gather.17.cloned.1.call-start = ((), (), s32[]{:S(2)}) async-start(), calls=%async_computation.6 | async-start | bytes 10485760 | tf_op jit(solution)/shard_map/all_gather | solution.py:68
  131.3 27.0 %copy-start.3 = (s32[256]{0:T(256)S(1)}, s32[256]{0:T(256)}, u32[]{:S(2)}) copy-start(s32[256]{0:T(256)} %param.15) | copy-start | bytes 3076
  139.8 18.4 %copy-start.1 = (f32[256,4096]{1,0:T(8,128)}, f32[256,4096]{1,0:T(8,128)S(1)}, u32[]{:S(2)}) copy-start(f32[256,4096]{1,0:T(8,128)S(1)} %get-tuple-element.72) | copy-start | bytes 12582916
  199.7 24.2 %all-to-all-start.1 = ((bf16[8,32,256]{2,1,0:T(8,128)(2,1)}), bf16[8,32,256]{2,1,0:T(8,128)(2,1)S(1)}, u32[]{:S(2)}, u32[]{:S(2)}) async-start(bf16[8,32,256]{2,1,0:T(8,128)(2,1)} %bitcast.11), calls=%async_computation.1 | async-start | bytes 262144 | tf_op jit(solution)/shard_map/all_to_all | solution.py:41
  217.5 12.6 %copy-start.2 = (f32[2048]{0:T(1024)S(1)}, f32[2048]{0:T(1024)}, u32[]{:S(2)}) copy-start(f32[2048]{0:T(1024)} %param.12) | copy-start | bytes 24580
  223.9 22.6 %all-to-all-start.2 = ((bf16[8,2,32768]{2,1,0:T(2,128)(2,1)}), bf16[8,2,32768]{2,1,0:T(2,128)(2,1)}, u32[]{:S(2)}, u32[]{:S(2)}) async-start(bf16[8,2,32768]{2,1,0:T(2,128)(2,1)} %reshape.76), calls=%async_computation.2 | async-start | bytes 2097152 | tf_op jit(solution)/shard_map/all_to_all | solution.py:75
Sparse Core Ops, SparseCore 0:
  10.2 60.0 all-gather.10
  94.5 36.6 all-gather.12
  132.8 33.4 all-gather.14
  199.8 55.4 all-gather.16
where the time goes:
time: 278 us; the launch traced here: 277 us
  waiting for transfers between devices  106 us (38%)
  blocking collectives  72 us (26%)
  matrix products  38 us (14%)
  starting transfers between devices  16.9 us (6%)
  local copies, waits for them, and re-layouts  16 us (6%)
  other arithmetic  14.3 us (5%)
  between operations  13.9 us (5%)
    all_gather x3, blocking collectives, combined_all(): pieces = jax.tree.map(lambda part: lax.all_gather(part, axis), value)  53 us
    all_gather x1, waiting for transfers between devices, body(): lax.all_gather(hidden, 'vp', axis=1, tiled=True)  45.9 us
    all_gather x1, waiting for transfers between devices, body(): normed = lax.all_gather(normed_cols, 'vp', axis=1, tiled=True)  36.7 us
    psum x1, blocking collectives, body(): square_total = lax.psum(jnp.sum(col_values * col_values, axis=1), 'vp')  19 us
    all_to_all x1, waiting for transfers between devices, body(): lax.all_to_all(row_term[:, None, :].astype(jnp.bfloat16), 'vp', split_axi...  15.8 us
    dot_general x1, matrix products, body(): lax.dot_general(dscore, vocab, (((1,), (1,)), ((), ())), preferred_elemen...  14.3 us
    unnamed x16, local copies, waits for them, and re-layouts  12.2 us
    dot_general x1, matrix products, body(): lax.dot_general(rows_slice, lax.all_gather(dscore, 'dp', axis=0, tiled=Tr...  11.7 us
  transfers between devices with their start and end apart: 7, of which 4 were waited for; matrix products, arithmetic and copies ran while one was open for 19% of the time, Pallas kernels for 0%

commit v1 on v0

--- a/solution.py
+++ b/solution.py
@@ -1,6 +1,10 @@
+import functools
+
 import jax
 import jax.numpy as jnp
 from jax import lax
+from jax.experimental import pallas as pl
+from jax.experimental.pallas import tpu as pltpu
 from jax.sharding import PartitionSpec as P
 
 norm_eps = 1e-06
@@ -83,6 +87,583 @@
     return (losses, grad_input, grad_vocab)
 
 
+MESH = pl.DeviceIdType.MESH
+HALVES = 2
+TILE = 512
+
+
+def send(src, dst, send_sem, recv_sem, vp, dp):
+    return pltpu.make_async_remote_copy(
+        src_ref=src,
+        dst_ref=dst,
+        send_sem=send_sem,
+        recv_sem=recv_sem,
+        device_id={"vp": vp, "dp": dp},
+        device_id_type=MESH,
+    )
+
+
+def gather(n, me, dp, own, place, sems, extra):
+    line = n // 2
+    row = me // 2
+    side = me - 2 * row
+    other = me + 1 - 2 * side
+    send_sem, recv_sem = sems
+
+    def copy(way, slot, part, target, src=None):
+        src = place(slot, part) if src is None else src
+        return send(
+            src,
+            place(slot, part),
+            send_sem.at[way, slot, part],
+            recv_sem.at[slot, part],
+            target,
+            dp,
+        )
+
+    for part in range(HALVES):
+        copy(0, me, part, other, own(part)).start()
+
+        @pl.when(row < line - 1)
+        def _():
+            copy(1, me, part, me + 2, own(part)).start()
+
+        @pl.when(row > 0)
+        def _():
+            copy(2, me, part, me - 2, own(part)).start()
+
+        extra(me, part)
+
+    def crossed(k):
+        for part in range(HALVES):
+            for step in (-k, k) if k else (0,):
+                slot = other + 2 * step
+
+                @pl.when((row + step >= 0) & (row + step < line))
+                def _():
+                    copy(0, slot, part, other).wait_recv()
+                    extra(slot, part)
+
+    for k in range(1, line):
+        for part in range(HALVES):
+            for step, way in ((-k, 1), (k, 2)):
+                slot = me + 2 * step
+
+                @pl.when((row + step >= 0) & (row + step < line))
+                def _():
+                    copy(0, slot, part, other).wait_recv()
+                    on = row < line - 1 if way == 1 else row > 0
+
+                    @pl.when(on)
+                    def _():
+                        copy(way, slot, part, me + 2 if way == 1 else me - 2).start()
+
+                    copy(0, slot, part, other).start()
+                    extra(slot, part)
+
+        crossed(k - 1)
+    crossed(line - 1)
+
+    def finish():
+        for part in range(HALVES):
+            copy(0, me, part, other, own(part)).wait_send()
+
+            @pl.when(row < line - 1)
+            def _():
+                copy(1, me, part, me + 2, own(part)).wait_send()
+
+            @pl.when(row > 0)
+            def _():
+                copy(2, me, part, me - 2, own(part)).wait_send()
+
+            for k in range(1, line):
+                for step, way in ((-k, 1), (k, 2)):
+                    slot = me + 2 * step
+
+                    @pl.when((row + step >= 0) & (row + step < line))
+                    def _():
+                        copy(0, slot, part, other).wait_send()
+
+                        @pl.when(row < line - 1 if way == 1 else row > 0)
+                        def _():
+                            copy(way, slot, part, me).wait_send()
+
+    return finish
+
+
+def head_kernel(
+    n,
+    hidden,
+    w_down,
+    stream,
+    gain,
+    vocab,
+    bias,
+    targets,
+    loss_out,
+    input_out,
+    vocab_out,
+    units,
+    stream_cols,
+    normin,
+    normed,
+    words,
+    scores,
+    tops,
+    lanes,
+    stats,
+    dscore,
+    slices,
+    flipped,
+    terms,
+    landed,
+    staged,
+    unit_send,
+    unit_recv,
+    norm_send,
+    norm_recv,
+    stream_send,
+    stream_recv,
+    twin_send,
+    twin_recv,
+    stat_send,
+    stat_recv,
+    score_send,
+    score_recv,
+    slice_send,
+    slice_recv,
+    term_send,
+    term_recv,
+    load_sem,
+    out_sem,
+):
+    me = lax.axis_index("vp")
+    dp = lax.axis_index("dp")
+    twin = lax.rem(dp + 2, 4)
+    core = lax.rem(dp, 2)
+    sibling = dp + 1 - 2 * core
+    group, depth = hidden.shape
+    width = gain.shape[1]
+    feats = stream_cols.shape[1]
+    rows_dev = stream.shape[0]
+    ncols = bias.shape[1]
+    own_feats = slices.shape[1]
+    half = group // HALVES
+
+    load = pltpu.make_async_copy(vocab, words, load_sem)
+    load.start()
+    barrier = pltpu.get_barrier_semaphore()
+
+    def greet(j, _):
+        peer = lax.rem(me + j, n)
+        pl.semaphore_signal(barrier, 1, device_id={"vp": peer, "dp": dp}, device_id_type=MESH)
+        pl.semaphore_signal(barrier, 1, device_id={"vp": peer, "dp": twin}, device_id_type=MESH)
+        return 0
+
+    lax.fori_loop(1, n, greet, 0)
+    pl.semaphore_signal(barrier, 1, device_id={"vp": me, "dp": twin}, device_id_type=MESH)
+    pl.semaphore_signal(barrier, 1, device_id={"vp": me, "dp": sibling}, device_id_type=MESH)
+    pl.semaphore_wait(barrier, 2 * n)
+
+    def stream_copy(j):
+        peer = lax.rem(me + j, n)
+        return send(
+            stream.at[:, pl.ds(pl.multiple_of(peer * feats, 128), feats)],
+            stream_cols.at[pl.ds(pl.multiple_of(me * rows_dev, rows_dev), rows_dev), :],
+            stream_send.at[j],
+            stream_recv.at[j],
+            peer,
+            dp,
+        )
+
+    def start_stream(j, _):
+        stream_copy(j).start()
+        return 0
+
+    def wait_stream(j, _):
+        stream_copy(j).wait()
+        return 0
+
+    units[me] = hidden[...]
+    stream_cols[pl.ds(pl.multiple_of(me * rows_dev, rows_dev), rows_dev), :] = stream[
+        :, pl.ds(pl.multiple_of(me * feats, 128), feats)
+    ]
+    lax.fori_loop(1, n, start_stream, 0)
+    finish_units = gather(
+        n,
+        me,
+        dp,
+        lambda part: hidden.at[pl.ds(part * half, half), :],
+        lambda slot, part: units.at[slot, pl.ds(part * half, half), :],
+        (unit_send, unit_recv),
+        lambda slot, part: None,
+    )
+    lax.fori_loop(1, n, wait_stream, 0)
+
+    def project(slot, total):
+        rows = pl.ds(pl.multiple_of(slot * depth, 16), depth)
+        return total + jnp.dot(units[slot], w_down[rows, :], preferred_element_type=jnp.float32)
+
+    proj = lax.fori_loop(0, n, project, jnp.zeros((group, feats), jnp.float32))
+
+    def cols_of(slot):
+        return pl.ds(pl.multiple_of(slot * feats, 128), feats)
+
+    normin[0, :, cols_of(me)] = (stream_cols[...].astype(jnp.float32) + proj).astype(jnp.bfloat16)
+
+    def twin_copy(slot, part):
+        rows = pl.ds(part * half, half)
+        return send(
+            normin.at[0, rows, cols_of(slot)],
+            normin.at[1, rows, cols_of(slot)],
+            twin_send.at[slot, part],
+            twin_recv.at[slot, part],
+            me,
+            twin,
+        )
+
+    finish_norm = gather(
+        n,
+        me,
+        dp,
+        lambda part: normin.at[0, pl.ds(part * half, half), cols_of(me)],
+        lambda slot, part: normin.at[0, pl.ds(part * half, half), cols_of(slot)],
+        (norm_send, norm_recv),
+        lambda slot, part: twin_copy(slot, part).start(),
+    )
+
+    def normalize(which):
+        def block(j, _):
+            rows = pl.ds(pl.multiple_of(j * 32, 32), 32)
+            values = normin[which, rows, :].astype(jnp.float32)
+            inv = lax.rsqrt(jnp.mean(values * values, axis=1, keepdims=True) + norm_eps)
+            normed[which, rows, :] = (values * inv * gain[...]).astype(jnp.bfloat16)
+            return 0
+
+        lax.fori_loop(0, group // 32, block, 0)
+
+    def slice_copy(which, home):
+        rows = pl.ds(pl.multiple_of(home * group, group), group)
+        cols = pl.ds(pl.multiple_of(sibling * own_feats, 128), own_feats)
+        return send(
+            normed.at[which, :, cols],
+            slices.at[rows, :],
+            slice_send.at[which],
+            slice_recv.at[which],
+            me,
+            sibling,
+        )
+
+    def folded(values, join):
+        result = values[:, :128]
+        for at in range(128, TILE, 128):
+            result = join(result, values[:, at : at + 128])
+        return result
+
+    def score(which):
+        tops[which] = jnp.full((group, 128), -jnp.inf, jnp.float32)
+
+        def block(j, _):
+            cols = pl.ds(pl.multiple_of(j * TILE, TILE), TILE)
+            values = (
+                jnp.dot(normed[which], words[:, cols], preferred_element_type=jnp.float32)
+                + bias[:, cols]
+            )
+            scores[which, :, cols] = values
+            tops[which] = jnp.maximum(tops[which], folded(values, jnp.maximum))
+            return 0
+
+        lax.fori_loop(0, ncols // TILE, block, 0)
+        top = jnp.max(tops[which], axis=1, keepdims=True)
+        tops[which] = jnp.broadcast_to(top, (group, 128))
+        lanes[...] = jnp.zeros_like(lanes)
+
+        def powers(j, _):
+            cols = pl.ds(pl.multiple_of(j * TILE, TILE), TILE)
+            values = scores[which, :, cols]
+            if which == 0:
+                ids = lax.broadcasted_iota(jnp.int32, (group, TILE), 1) + (me * ncols + j * TILE)
+                hits = jnp.where(ids == targets[...], values, 0.0)
+                lanes[1] += folded(hits, jnp.add)
+            values = jnp.exp(values - top)
+            scores[which, :, cols] = values
+            if which == 0:
+                lanes[0] += folded(values, jnp.add)
+            return 0
+
+        lax.fori_loop(0, ncols // TILE, powers, 0)
+        return top
+
+    def stat_copy(away, j, home):
+        peer = lax.rem(me + j, n)
+        return send(
+            stats.at[0, me],
+            stats.at[away, me],
+            stat_send.at[away, j],
+            stat_recv.at[away, j],
+            peer,
+            home,
+        )
+
+    normalize(0)
+    load.wait()
+    slice_copy(0, dp).start()
+    top = score(0)
+    lane = lax.broadcasted_iota(jnp.int32, (group, 128), 1)
+    packed = jnp.where(
+        lane == 0,
+        top,
+        jnp.where(
+            lane == 1,
+            jnp.sum(lanes[0], axis=1, keepdims=True),
+            jnp.where(
+                lane == 2,
+                jnp.sum(lanes[1], axis=1, keepdims=True),
+                jnp.where(lane == 3, targets[...].astype(jnp.float32), 0.0),
+            ),
+        ),
+    )
+    stats[0, me] = jnp.transpose(packed)[:8, :]
+
+    def start_stats(j, _):
+        stat_copy(0, j, dp).start()
+        stat_copy(1, j, twin).start()
+        return 0
+
+    def wait_stats(j, _):
+        stat_copy(0, j, dp).wait()
+        stat_copy(1, j, twin).wait()
+        return 0
+
+    stat_copy(1, 0, twin).start()
+    lax.fori_loop(1, n, start_stats, 0)
+
+    for slot in range(n):
+        for part in range(HALVES):
+            twin_copy(slot, part).wait()
+    normalize(1)
+    slice_copy(1, twin).start()
+    score(1)
+    stat_copy(1, 0, twin).wait()
+    lax.fori_loop(1, n, wait_stats, 0)
+
+    def score_copy(which, home):
+        rows = pl.ds(pl.multiple_of(home * group, group), group)
+        return send(
+            dscore.at[rows, :],
+            dscore.at[rows, :],
+            score_send.at[which],
+            score_recv.at[which],
+            me,
+            sibling,
+        )
+
+    def derive(which, home):
+        parts = stats[which]
+        highest = jnp.max(parts[:, 0, :], axis=0, keepdims=True)
+        total = jnp.sum(parts[:, 1, :] * jnp.exp(parts[:, 0, :] - highest), axis=0, keepdims=True)
+        lse = highest + jnp.log(total)
+        if which == 0:
+            goal = jnp.sum(parts[:, 2, :], axis=0, keepdims=True)
+            loss_out[...] = lse - goal + zloss_weight * lse * lse
+        level = lax.broadcasted_iota(jnp.int32, (128, group), 0)
+        turned = jnp.transpose(
+            jnp.where(level == 0, lse, jnp.where(level == 1, parts[0, 3:4, :], 0.0))
+        )
+        lse_col = turned[:, 0:1]
+        goal_col = turned[:, 1:2].astype(jnp.int32)
+        factor = jnp.exp(tops[which][:, 0:1] - lse_col) * (1.0 + 2.0 * zloss_weight * lse_col)
+        rows = pl.ds(pl.multiple_of(home * group, group), group)
+
+        def block(j, _):
+            cols = pl.ds(pl.multiple_of(j * TILE, TILE), TILE)
+            ids = lax.broadcasted_iota(jnp.int32, (group, TILE), 1) + (me * ncols + j * TILE)
+            values = scores[which, :, cols] * factor - jnp.where(ids == goal_col, 1.0, 0.0)
+            dscore[rows, cols] = values.astype(jnp.bfloat16)
+            return 0
+
+        lax.fori_loop(0, ncols // TILE, block, 0)
+        score_copy(which, home).start()
+
+    derive(0, dp)
+    derive(1, twin)
+
+    def term_copy(t, j):
+        peer = lax.rem(me + j, n)
+        cols = pl.ds(pl.multiple_of(t * TILE, TILE), TILE)
+        return send(
+            terms.at[pl.ds(pl.multiple_of(peer * rows_dev, rows_dev), rows_dev), cols],
+            landed.at[me, :, cols],
+            term_send.at[t, j],
+            term_recv.at[t, j],
+            peer,
+            dp,
+        )
+
+    own_rows = pl.ds(pl.multiple_of(dp * group, group), group)
+
+    def term_block(t, _):
+        cols = pl.ds(pl.multiple_of(t * TILE, TILE), TILE)
+        terms[:, cols] = lax.dot_general(
+            dscore[own_rows, :],
+            words[cols, :],
+            (((1,), (1,)), ((), ())),
+            preferred_element_type=jnp.float32,
+        ).astype(jnp.bfloat16)
+
+        def start(j, _):
+            term_copy(t, j).start()
+            return 0
+
+        return lax.fori_loop(1, n, start, 0)
+
+    lax.fori_loop(0, width // TILE, term_block, 0)
+    my_rows = pl.ds(pl.multiple_of(me * rows_dev, rows_dev), rows_dev)
+    landed[me] = terms[my_rows, :]
+
+    for which, home in ((0, dp), (1, twin)):
+        rows = pl.ds(pl.multiple_of(home * group, group), group)
+        slices[rows, :] = normed[which, :, pl.ds(pl.multiple_of(dp * own_feats, 128), own_feats)]
+        slice_copy(which, home).wait()
+        score_copy(which, home).wait()
+    flipped[...] = jnp.transpose(slices[...])
+
+    def out_copy(j):
+        slot = lax.rem(j, 2)
+        cols = pl.ds(pl.multiple_of(j * TILE, TILE), TILE)
+        return pltpu.make_async_copy(staged.at[slot], vocab_out.at[:, cols], out_sem.at[slot])
+
+    def vocab_block(j, _):
+        @pl.when(j >= 2)
+        def _():
+            out_copy(j - 2).wait()
+
+        cols = pl.ds(pl.multiple_of(j * TILE, TILE), TILE)
+        staged[lax.rem(j, 2)] = jnp.dot(
+            flipped[...], dscore[:, cols], preferred_element_type=jnp.float32
+        )
+        out_copy(j).start()
+        return 0
+
+    blocks = ncols // TILE
+    lax.fori_loop(0, blocks, vocab_block, 0)
+
+    def wait_terms(t, _):
+        def wait(j, _):
+            term_copy(t, j).wait()
+            return 0
+
+        return lax.fori_loop(1, n, wait, 0)
+
+    lax.fori_loop(0, width // TILE, wait_terms, 0)
+    values = normin[0, my_rows, :].astype(jnp.float32)
+    inv = lax.rsqrt(jnp.mean(values * values, axis=1, keepdims=True) + norm_eps)
+    dnormed = landed[0].astype(jnp.float32)
+    for slot in range(1, n):
+        dnormed += landed[slot].astype(jnp.float32)
+    scaled = dnormed * gain[...]
+    input_out[...] = inv * (
+        scaled - values * inv * inv * jnp.mean(values * scaled, axis=1, keepdims=True)
+    )
+    for j in range(max(blocks - 2, 0), blocks):
+        out_copy(j).wait()
+    finish_units()
+    finish_norm()
+
+
+def fused(stream, hidden, w_down, final_gain, vocab, vocab_bias, targets):
+    n = lax.axis_size("vp")
+    groups = lax.axis_size("dp")
+    rows_dev, width = stream.shape
+    group, depth = hidden.shape
+    feats = w_down.shape[1]
+    ncols = vocab.shape[1]
+    own_feats = width // groups
+    f32, bf16 = jnp.float32, jnp.bfloat16
+    dma = pltpu.SemaphoreType.DMA
+    vmem = pl.BlockSpec(memory_space=pltpu.VMEM)
+    hbm = pl.BlockSpec(memory_space=pl.ANY)
+    group_losses, grad_input, grad_vocab = pl.pallas_call(
+        functools.partial(head_kernel, n),
+        out_shape=(
+            jax.ShapeDtypeStruct((1, group), f32),
+            jax.ShapeDtypeStruct((rows_dev, width), f32),
+            jax.ShapeDtypeStruct((own_feats, ncols), f32),
+        ),
+        in_specs=[vmem, vmem, vmem, vmem, hbm, vmem, vmem],
+        out_specs=(vmem, vmem, hbm),
+        scratch_shapes=[
+            pltpu.VMEM((n, group, depth), bf16),
+            pltpu.VMEM((group, feats), bf16),
+            pltpu.VMEM((2, group, width), bf16),
+            pltpu.VMEM((2, group, width), bf16),
+            pltpu.VMEM((width, ncols), bf16),
+            pltpu.VMEM((2, group, ncols), f32),
+            pltpu.VMEM((2, group, 128), f32),
+            pltpu.VMEM((2, group, 128), f32),
+            pltpu.VMEM((2, n, 8, group), f32),
+            pltpu.VMEM((groups * group, ncols), bf16),
+            pltpu.VMEM((groups * group, own_feats), bf16),
+            pltpu.VMEM((own_feats, groups * group), bf16),
+            pltpu.VMEM((group, width), bf16),
+            pltpu.VMEM((n, rows_dev, width), bf16),
+            pltpu.VMEM((2, own_feats, TILE), f32),
+            dma((3, n, HALVES)),
+            dma((n, HALVES)),
+            dma((3, n, HALVES)),
+            dma((n, HALVES)),
+            dma((n,)),
+            dma((n,)),
+            dma((n, HALVES)),
+            dma((n, HALVES)),
+            dma((2, n)),
+            dma((2, n)),
+            dma((2,)),
+            dma((2,)),
+            dma((2,)),
+            dma((2,)),
+            dma((width // TILE, n)),
+            dma((width // TILE, n)),
+            dma,
+            dma((2,)),
+        ],
+        compiler_params=pltpu.CompilerParams(
+            collective_id=0, has_side_effects=True, vmem_limit_bytes=64 * 1024 * 1024 - 65536
+        ),
+    )(
+        hidden,
+        w_down,
+        stream,
+        final_gain.reshape(1, width),
+        vocab,
+        vocab_bias.reshape(1, ncols),
+        targets.reshape(group, 1),
+    )
+    losses = lax.dynamic_slice_in_dim(
+        group_losses.reshape(group), lax.axis_index("vp") * rows_dev, rows_dev
+    )
+    return (losses, grad_input, grad_vocab)
+
+
+def choose(stream, hidden, w_down, final_gain, vocab, vocab_bias, targets):
+    rows_dev, width = stream.shape
+    group, depth = hidden.shape
+    n, groups = lax.axis_size("vp"), lax.axis_size("dp")
+    tiles = (
+        n % 2 == 0
+        and groups == 4
+        and rows_dev % 32 == 0
+        and depth % 16 == 0
+        and group % (32 * HALVES) == 0
+        and w_down.shape[1] % 128 == 0
+        and width % TILE == 0
+        and (width // groups) % 128 == 0
+        and vocab.shape[1] % TILE == 0
+    )
+    path = fused if tiles else body
+    return path(stream, hidden, w_down, final_gain, vocab, vocab_bias, targets)
+
+
 def solution(mesh):
     placed = (
         P(("dp", "vp"), None),
@@ -94,7 +675,7 @@
         P("dp"),
     )
     return jax.shard_map(
-        body,
+        choose,
         mesh=mesh,
         in_specs=placed,
         out_specs=(P(("dp", "vp")), P(("dp", "vp"), None), P("dp", "vp")),

time: 278 us -> 123 us (0.44)
  Pallas kernels: 0 us -> 108 us
  waiting for transfers between devices: 106 us -> 0 us
  blocking collectives: 72 us -> 0 us
  matrix products: 38 us -> 0 us
  starting transfers between devices: 16.9 us -> 0 us
  other arithmetic: 14.3 us -> 0 us
  between operations: 13.9 us -> 0.65 us
    pallas_call x0 -> x1, Pallas kernels: none -> 108 us  [fused(): pl.pallas_call(functools.partial(head_kernel, n), out_shape=(jax.ShapeDty...]
    all_gather x4 -> x0, waiting for transfers between devices: 82.6 us -> none  [the longest x1 45.9 us: body(): lax.all_gather(hidden, 'vp', axis=1, tiled=True)]
    all_gather x3 -> x0, blocking collectives: 53 us -> none  [combined_all(): pieces = jax.tree.map(lambda part: lax.all_gather(part, axis), value)]
    dot_general x4 -> x0, matrix products: 38 us -> none  [the longest x1 14.3 us: body(): lax.dot_general(dscore, vocab, (((1,), (1,)), ((), ())), preferred_elemen...]
    all_to_all x3 -> x0, waiting for transfers between devices: 22.4 us -> none  [the longest x1 15.8 us: body(): lax.all_to_all(row_term[:, None, :].astype(jnp.bfloat16), 'vp', split_axi...]
    psum x1 -> x0, blocking collectives: 19 us -> none  [body(): square_total = lax.psum(jnp.sum(col_values * col_values, axis=1), 'vp')]
    all_to_all x3 -> x0, starting transfers between devices: 16.8 us -> none  [the longest x1 7.28 us: body(): lax.all_to_all(stream, 'vp', split_axis=1, concat_axis=0, tiled=True)]
    convert_element_type x4 -> x0, other arithmetic: 9.97 us -> none  [the longest x1 4.93 us: body(): (probs * (1.0 + 2.0 * zloss_weight * lse)[:, None] - jnp.where(hit, 1.0,...]
  transfers between devices with their start and end apart: 7 -> 0, of which waited for: 4 -> 0; matrix products, arithmetic and copies ran while one was open for 19% -> 0% of each run, Pallas kernels for 0% -> 0%
where the time goes in v1:
time: 123 us; the launch traced here: 122 us
  Pallas kernels  108 us (88%)
  local copies, waits for them, and re-layouts  14 us (11%)
    pallas_call x1, Pallas kernels, fused(): pl.pallas_call(functools.partial(head_kernel, n), out_shape=(jax.ShapeDty...  108 us
    unnamed x3, local copies, waits for them, and re-layouts  11.3 us

profile of v1, /device:TPU:0, one launch (start us, length us, event | category | flops | bytes accessed | tf_op | source)
XLA Modules:
  0.0 122.4 jit_solution(7637568974087483873)
XLA Ops:
  0.6 1.5 %copy.12.targets = s32[256,1]{1,0:T(8,128)} copy(s32[256,1]{0,1:T(1,128)} %bitcast.7) | data formatting | bytes 2048 | tf_op jit(solution)/shard_map/reshape | solution.py:640
  2.1 1.9 %copy.11.hidden = bf16[256,704]{1,0:T(8,128)(2,1)} copy(bf16[256,704]{0,1:T(8,128)(2,1)} %param.8) | data formatting | bytes 720896 | tf_op args[1]
  4.0 107.7 %shard_map.94 = (f32[1,256]{1,0:T(1,128)}, f32[32,2048]{1,0:T(8,128)}, f32[512,4096]{1,0:T(8,128)}) custom-call(bf16[256,704]{1,0:T(8,128)(2,1)} %copy.11.hidden, bf16[5632,256]{1,0:T(8,128)(2,1)} %w_down.1, bf16[32,2048]{1,0:T(8,128)(2,1)} %stream.1, f32[1,2048]{1,0:T(1,128)} %bitcast.6, bf16[2048,4096]{1,0:T(8,128)(2,1)} %vocab.1, f32[1,4096]{1,0:T(1,128)} %bitcast.5, ...), custom_call_target="tpu_custom_call" | custom-call | tf_op jit(solution)/shard_map/pallas_call | solution.py:586
  111.7 1.2 dynamic-slice_bitcast_fusion
  112.9 1.7 %copy.15 = f32[32,2048]{1,0:T(8,128)} copy(f32[32,2048]{1,0:T(8,128)} %get-tuple-element.13) | data formatting | bytes 524288
  114.6 7.8 %copy.16 = f32[512,4096]{1,0:T(8,128)} copy(f32[512,4096]{1,0:T(8,128)} %get-tuple-element.14) | data formatting | bytes 16777216

commit v2 on v1

--- a/solution.py
+++ b/solution.py
@@ -103,7 +103,7 @@
     )
 
 
-def gather(n, me, dp, own, place, sems, extra):
+def gather(n, me, dp, own, place, sems, extra, use):
     line = n // 2
     row = me // 2
     side = me - 2 * row
@@ -133,6 +133,7 @@
             copy(2, me, part, me - 2, own(part)).start()
 
         extra(me, part)
+    use(me)
 
     def crossed(k):
         for part in range(HALVES):
@@ -144,6 +145,13 @@
                     copy(0, slot, part, other).wait_recv()
                     extra(slot, part)
 
+    def used(k):
+        for step in (-k, k) if k else (0,):
+
+            @pl.when((row + step >= 0) & (row + step < line))
+            def _():
+                use(other + 2 * step)
+
     for k in range(1, line):
         for part in range(HALVES):
             for step, way in ((-k, 1), (k, 2)):
@@ -162,7 +170,15 @@
                     extra(slot, part)
 
         crossed(k - 1)
+        for step in (-k, k):
+
+            @pl.when((row + step >= 0) & (row + step < line))
+            def _():
+                use(me + 2 * step)
+
+        used(k - 1)
     crossed(line - 1)
+    used(line - 1)
 
     def finish():
         for part in range(HALVES):
@@ -202,7 +218,8 @@
     targets,
     loss_out,
     input_out,
-    vocab_out,
+    score_out,
+    flip_out,
     units,
     stream_cols,
     normin,
@@ -212,12 +229,12 @@
     tops,
     lanes,
     stats,
+    goals,
+    total,
     dscore,
     slices,
-    flipped,
     terms,
     landed,
-    staged,
     unit_send,
     unit_recv,
     norm_send,
@@ -235,6 +252,7 @@
     term_send,
     term_recv,
     load_sem,
+    unit_sem,
     out_sem,
 ):
     me = lax.axis_index("vp")
@@ -242,16 +260,21 @@
     twin = lax.rem(dp + 2, 4)
     core = lax.rem(dp, 2)
     sibling = dp + 1 - 2 * core
-    group, depth = hidden.shape
+    depth, group = hidden.shape
     width = gain.shape[1]
     feats = stream_cols.shape[1]
     rows_dev = stream.shape[0]
     ncols = bias.shape[1]
     own_feats = slices.shape[1]
     half = group // HALVES
+    piece = depth // HALVES
 
     load = pltpu.make_async_copy(vocab, words, load_sem)
+    bring = pltpu.make_async_copy(hidden, units.at[me], unit_sem)
+    bring.start()
     load.start()
+    goals[...] = jnp.transpose(jnp.broadcast_to(targets[...].astype(jnp.float32), (128, group)))
+    total[...] = jnp.zeros_like(total)
     barrier = pltpu.get_barrier_semaphore()
 
     def greet(j, _):
@@ -284,32 +307,39 @@
         stream_copy(j).wait()
         return 0
 
-    units[me] = hidden[...]
+    bring.wait()
     stream_cols[pl.ds(pl.multiple_of(me * rows_dev, rows_dev), rows_dev), :] = stream[
         :, pl.ds(pl.multiple_of(me * feats, 128), feats)
     ]
     lax.fori_loop(1, n, start_stream, 0)
+    def place_units(slot, part):
+        return units.at[slot, pl.ds(part * piece, piece), :]
+
+    def project(slot):
+        rows = pl.ds(pl.multiple_of(slot * depth, 16), depth)
+        total[...] += lax.dot_general(
+            units[slot],
+            w_down[rows, :],
+            (((0,), (0,)), ((), ())),
+            preferred_element_type=jnp.float32,
+        )
+
     finish_units = gather(
         n,
         me,
         dp,
-        lambda part: hidden.at[pl.ds(part * half, half), :],
-        lambda slot, part: units.at[slot, pl.ds(part * half, half), :],
+        lambda part: place_units(me, part),
+        place_units,
         (unit_send, unit_recv),
         lambda slot, part: None,
+        project,
     )
     lax.fori_loop(1, n, wait_stream, 0)
-
-    def project(slot, total):
-        rows = pl.ds(pl.multiple_of(slot * depth, 16), depth)
-        return total + jnp.dot(units[slot], w_down[rows, :], preferred_element_type=jnp.float32)
-
-    proj = lax.fori_loop(0, n, project, jnp.zeros((group, feats), jnp.float32))
 
     def cols_of(slot):
         return pl.ds(pl.multiple_of(slot * feats, 128), feats)
 
-    normin[0, :, cols_of(me)] = (stream_cols[...].astype(jnp.float32) + proj).astype(jnp.bfloat16)
+    normin[0, :, cols_of(me)] = (stream_cols[...].astype(jnp.float32) + total[...]).astype(jnp.bfloat16)
 
     def twin_copy(slot, part):
         rows = pl.ds(part * half, half)
@@ -330,6 +360,7 @@
         lambda slot, part: normin.at[0, pl.ds(part * half, half), cols_of(slot)],
         (norm_send, norm_recv),
         lambda slot, part: twin_copy(slot, part).start(),
+        lambda slot: None,
     )
 
     def normalize(which):
@@ -360,9 +391,7 @@
             result = join(result, values[:, at : at + 128])
         return result
 
-    def score(which):
-        tops[which] = jnp.full((group, 128), -jnp.inf, jnp.float32)
-
+    def score(which, first, last):
         def block(j, _):
             cols = pl.ds(pl.multiple_of(j * TILE, TILE), TILE)
             values = (
@@ -373,7 +402,9 @@
             tops[which] = jnp.maximum(tops[which], folded(values, jnp.maximum))
             return 0
 
-        lax.fori_loop(0, ncols // TILE, block, 0)
+        lax.fori_loop(first, last, block, 0)
+
+    def level(which):
         top = jnp.max(tops[which], axis=1, keepdims=True)
         tops[which] = jnp.broadcast_to(top, (group, 128))
         lanes[...] = jnp.zeros_like(lanes)
@@ -383,7 +414,7 @@
             values = scores[which, :, cols]
             if which == 0:
                 ids = lax.broadcasted_iota(jnp.int32, (group, TILE), 1) + (me * ncols + j * TILE)
-                hits = jnp.where(ids == targets[...], values, 0.0)
+                hits = jnp.where(ids == own_goals, values, 0.0)
                 lanes[1] += folded(hits, jnp.add)
             values = jnp.exp(values - top)
             scores[which, :, cols] = values
@@ -405,10 +436,15 @@
             home,
         )
 
+    tops[...] = jnp.full(tops.shape, -jnp.inf, jnp.float32)
+    own_goals = goals[:, 0:1].astype(jnp.int32)
+    blocks = ncols // TILE
+    middle = blocks // 2
     normalize(0)
     load.wait()
     slice_copy(0, dp).start()
-    top = score(0)
+    score(0, 0, blocks)
+    top = level(0)
     lane = lax.broadcasted_iota(jnp.int32, (group, 128), 1)
     packed = jnp.where(
         lane == 0,
@@ -419,7 +455,7 @@
             jnp.where(
                 lane == 2,
                 jnp.sum(lanes[1], axis=1, keepdims=True),
-                jnp.where(lane == 3, targets[...].astype(jnp.float32), 0.0),
+                jnp.where(lane == 3, goals[...], 0.0),
             ),
         ),
     )
@@ -428,11 +464,6 @@
     def start_stats(j, _):
         stat_copy(0, j, dp).start()
         stat_copy(1, j, twin).start()
-        return 0
-
-    def wait_stats(j, _):
-        stat_copy(0, j, dp).wait()
-        stat_copy(1, j, twin).wait()
         return 0
 
     stat_copy(1, 0, twin).start()
@@ -443,20 +474,29 @@
             twin_copy(slot, part).wait()
     normalize(1)
     slice_copy(1, twin).start()
-    score(1)
-    stat_copy(1, 0, twin).wait()
-    lax.fori_loop(1, n, wait_stats, 0)
+    score(1, 0, middle)
+
+    def wait_stats(away, home):
+        def wait(j, _):
+            stat_copy(away, j, home).wait()
+            return 0
+
+        lax.fori_loop(1, n, wait, 0)
 
     def score_copy(which, home):
         rows = pl.ds(pl.multiple_of(home * group, group), group)
         return send(
-            dscore.at[rows, :],
-            dscore.at[rows, :],
+            dscore.at[which],
+            score_out.at[rows, :],
             score_send.at[which],
             score_recv.at[which],
             me,
             sibling,
         )
+
+    def keep_copy(which, home):
+        rows = pl.ds(pl.multiple_of(home * group, group), group)
+        return pltpu.make_async_copy(dscore.at[which], score_out.at[rows, :], out_sem.at[which])
 
     def derive(which, home):
         parts = stats[which]
@@ -465,28 +505,28 @@
         lse = highest + jnp.log(total)
         if which == 0:
             goal = jnp.sum(parts[:, 2, :], axis=0, keepdims=True)
-            loss_out[...] = lse - goal + zloss_weight * lse * lse
-        level = lax.broadcasted_iota(jnp.int32, (128, group), 0)
+            loss_out[...] = jnp.broadcast_to(lse - goal + zloss_weight * lse * lse, (8, group))
+        line = lax.broadcasted_iota(jnp.int32, (128, group), 0)
         turned = jnp.transpose(
-            jnp.where(level == 0, lse, jnp.where(level == 1, parts[0, 3:4, :], 0.0))
+            jnp.where(line == 0, lse, jnp.where(line == 1, parts[0, 3:4, :], 0.0))
         )
         lse_col = turned[:, 0:1]
         goal_col = turned[:, 1:2].astype(jnp.int32)
         factor = jnp.exp(tops[which][:, 0:1] - lse_col) * (1.0 + 2.0 * zloss_weight * lse_col)
-        rows = pl.ds(pl.multiple_of(home * group, group), group)
 
         def block(j, _):
             cols = pl.ds(pl.multiple_of(j * TILE, TILE), TILE)
             ids = lax.broadcasted_iota(jnp.int32, (group, TILE), 1) + (me * ncols + j * TILE)
             values = scores[which, :, cols] * factor - jnp.where(ids == goal_col, 1.0, 0.0)
-            dscore[rows, cols] = values.astype(jnp.bfloat16)
+            dscore[which, :, cols] = values.astype(jnp.bfloat16)
             return 0
 
         lax.fori_loop(0, ncols // TILE, block, 0)
         score_copy(which, home).start()
-
+        keep_copy(which, home).start()
+
+    wait_stats(0, dp)
     derive(0, dp)
-    derive(1, twin)
 
     def term_copy(t, j):
         peer = lax.rem(me + j, n)
@@ -500,12 +540,10 @@
             dp,
         )
 
-    own_rows = pl.ds(pl.multiple_of(dp * group, group), group)
-
     def term_block(t, _):
         cols = pl.ds(pl.multiple_of(t * TILE, TILE), TILE)
         terms[:, cols] = lax.dot_general(
-            dscore[own_rows, :],
+            dscore[0],
             words[cols, :],
             (((1,), (1,)), ((), ())),
             preferred_element_type=jnp.float32,
@@ -520,33 +558,17 @@
     lax.fori_loop(0, width // TILE, term_block, 0)
     my_rows = pl.ds(pl.multiple_of(me * rows_dev, rows_dev), rows_dev)
     landed[me] = terms[my_rows, :]
+    score(1, middle, blocks)
+    level(1)
+    stat_copy(1, 0, twin).wait()
+    wait_stats(1, twin)
+    derive(1, twin)
 
     for which, home in ((0, dp), (1, twin)):
         rows = pl.ds(pl.multiple_of(home * group, group), group)
         slices[rows, :] = normed[which, :, pl.ds(pl.multiple_of(dp * own_feats, 128), own_feats)]
         slice_copy(which, home).wait()
-        score_copy(which, home).wait()
-    flipped[...] = jnp.transpose(slices[...])
-
-    def out_copy(j):
-        slot = lax.rem(j, 2)
-        cols = pl.ds(pl.multiple_of(j * TILE, TILE), TILE)
-        return pltpu.make_async_copy(staged.at[slot], vocab_out.at[:, cols], out_sem.at[slot])
-
-    def vocab_block(j, _):
-        @pl.when(j >= 2)
-        def _():
-            out_copy(j - 2).wait()
-
-        cols = pl.ds(pl.multiple_of(j * TILE, TILE), TILE)
-        staged[lax.rem(j, 2)] = jnp.dot(
-            flipped[...], dscore[:, cols], preferred_element_type=jnp.float32
-        )
-        out_copy(j).start()
-        return 0
-
-    blocks = ncols // TILE
-    lax.fori_loop(0, blocks, vocab_block, 0)
+    flip_out[...] = jnp.transpose(slices[...])
 
     def wait_terms(t, _):
         def wait(j, _):
@@ -565,10 +587,23 @@
     input_out[...] = inv * (
         scaled - values * inv * inv * jnp.mean(values * scaled, axis=1, keepdims=True)
     )
-    for j in range(max(blocks - 2, 0), blocks):
-        out_copy(j).wait()
+    for which, home in ((0, dp), (1, twin)):
+        keep_copy(which, home).wait()
+        score_copy(which, home).wait()
     finish_units()
     finish_norm()
+
+
+def vocab_kernel(flipped, dscore, grad_input, losses, vocab_out, input_out, loss_out):
+    rows_dev = loss_out.shape[1]
+    group = losses.shape[1]
+    vocab_out[...] = jnp.dot(flipped[...], dscore[...], preferred_element_type=jnp.float32)
+
+    @pl.when(pl.program_id(0) == 0)
+    def _():
+        input_out[...] = grad_input[...]
+        shift = lax.rem(group - lax.axis_index("vp") * rows_dev, group)
+        loss_out[...] = pltpu.roll(losses[...], shift, 1)[0:1, :rows_dev]
 
 
 def fused(stream, hidden, w_down, final_gain, vocab, vocab_bias, targets):
@@ -579,21 +614,23 @@
     feats = w_down.shape[1]
     ncols = vocab.shape[1]
     own_feats = width // groups
+    tokens = groups * group
     f32, bf16 = jnp.float32, jnp.bfloat16
     dma = pltpu.SemaphoreType.DMA
     vmem = pl.BlockSpec(memory_space=pltpu.VMEM)
     hbm = pl.BlockSpec(memory_space=pl.ANY)
-    group_losses, grad_input, grad_vocab = pl.pallas_call(
+    group_losses, grad_input, dscore, flipped = pl.pallas_call(
         functools.partial(head_kernel, n),
         out_shape=(
-            jax.ShapeDtypeStruct((1, group), f32),
+            jax.ShapeDtypeStruct((8, group), f32),
             jax.ShapeDtypeStruct((rows_dev, width), f32),
-            jax.ShapeDtypeStruct((own_feats, ncols), f32),
+            jax.ShapeDtypeStruct((tokens, ncols), bf16),
+            jax.ShapeDtypeStruct((own_feats, tokens), bf16),
         ),
-        in_specs=[vmem, vmem, vmem, vmem, hbm, vmem, vmem],
-        out_specs=(vmem, vmem, hbm),
+        in_specs=[hbm, vmem, vmem, vmem, hbm, vmem, vmem],
+        out_specs=(vmem, vmem, hbm, vmem),
         scratch_shapes=[
-            pltpu.VMEM((n, group, depth), bf16),
+            pltpu.VMEM((n, depth, group), bf16),
             pltpu.VMEM((group, feats), bf16),
             pltpu.VMEM((2, group, width), bf16),
             pltpu.VMEM((2, group, width), bf16),
@@ -602,12 +639,12 @@
             pltpu.VMEM((2, group, 128), f32),
             pltpu.VMEM((2, group, 128), f32),
             pltpu.VMEM((2, n, 8, group), f32),
-            pltpu.VMEM((groups * group, ncols), bf16),
-            pltpu.VMEM((groups * group, own_feats), bf16),
-            pltpu.VMEM((own_feats, groups * group), bf16),
+            pltpu.VMEM((group, 128), f32),
+            pltpu.VMEM((group, feats), f32),
+            pltpu.VMEM((2, group, ncols), bf16),
+            pltpu.VMEM((tokens, own_feats), bf16),
             pltpu.VMEM((group, width), bf16),
             pltpu.VMEM((n, rows_dev, width), bf16),
-            pltpu.VMEM((2, own_feats, TILE), f32),
             dma((3, n, HALVES)),
             dma((n, HALVES)),
             dma((3, n, HALVES)),
@@ -625,24 +662,46 @@
             dma((width // TILE, n)),
             dma((width // TILE, n)),
             dma,
+            dma,
             dma((2,)),
         ],
         compiler_params=pltpu.CompilerParams(
             collective_id=0, has_side_effects=True, vmem_limit_bytes=64 * 1024 * 1024 - 65536
         ),
     )(
-        hidden,
+        hidden.T,
         w_down,
         stream,
         final_gain.reshape(1, width),
         vocab,
         vocab_bias.reshape(1, ncols),
-        targets.reshape(group, 1),
-    )
-    losses = lax.dynamic_slice_in_dim(
-        group_losses.reshape(group), lax.axis_index("vp") * rows_dev, rows_dev
-    )
-    return (losses, grad_input, grad_vocab)
+        targets.reshape(1, group),
+    )
+
+    def whole(*shape):
+        return pl.BlockSpec(shape, lambda j: (0, 0))
+
+    grad_vocab, grad_input, losses = pl.pallas_call(
+        vocab_kernel,
+        grid=(ncols // TILE,),
+        out_shape=(
+            jax.ShapeDtypeStruct((own_feats, ncols), f32),
+            jax.ShapeDtypeStruct((rows_dev, width), f32),
+            jax.ShapeDtypeStruct((1, rows_dev), f32),
+        ),
+        in_specs=[
+            whole(own_feats, tokens),
+            pl.BlockSpec((tokens, TILE), lambda j: (0, j)),
+            whole(rows_dev, width),
+            whole(8, group),
+        ],
+        out_specs=(
+            pl.BlockSpec((own_feats, TILE), lambda j: (0, j)),
+            whole(rows_dev, width),
+            whole(1, rows_dev),
+        ),
+    )(flipped, dscore, grad_input, group_losses)
+    return (losses.reshape(rows_dev), grad_input, grad_vocab)
 
 
 def choose(stream, hidden, w_down, final_gain, vocab, vocab_bias, targets):
@@ -653,7 +712,7 @@
         n % 2 == 0
         and groups == 4
         and rows_dev % 32 == 0
-        and depth % 16 == 0
+        and depth % (16 * HALVES) == 0
         and group % (32 * HALVES) == 0
         and w_down.shape[1] % 128 == 0
         and width % TILE == 0

time: 123 us -> 111 us (0.902)
  local copies, waits for them, and re-layouts: 14 us -> 0 us
  Pallas kernels: 108 us -> 110 us
    unnamed x3 -> x0, local copies, waits for them, and re-layouts: 11.3 us -> none
    pallas_call x0 -> x1, Pallas kernels: none -> 11.3 us  [fused(): pl.pallas_call(vocab_kernel, grid=(ncols // TILE,), out_shape=(jax.ShapeD...]
    pallas_call x1, Pallas kernels: 108 us -> 98.4 us  [fused(): pl.pallas_call(functools.partial(head_kernel, n), out_shape=(jax.ShapeDty...]
    reshape x1 -> x0, local copies, waits for them, and re-layouts: 1.47 us -> none  [fused(): targets.reshape(group, 1)]
where the time goes in v2:
time: 111 us; the launch traced here: 110 us
  Pallas kernels  110 us (99%)
    pallas_call x1, Pallas kernels, fused(): pl.pallas_call(functools.partial(head_kernel, n), out_shape=(jax.ShapeDty...  98.4 us
    pallas_call x1, Pallas kernels, fused(): pl.pallas_call(vocab_kernel, grid=(ncols // TILE,), out_shape=(jax.ShapeD...  11.3 us

profile of v2, /device:TPU:0, one launch (start us, length us, event | category | flops | bytes accessed | tf_op | source)
XLA Modules:
  0.0 110.4 jit_solution(112721965959320709)
XLA Ops:
  0.6 98.4 %shard_map.94 = (f32[8,256]{1,0:T(8,128)}, f32[32,2048]{1,0:T(8,128)}, bf16[1024,4096]{1,0:T(8,128)(2,1)}, bf16[512,1024]{1,0:T(8,128)(2,1)}) custom-call(bf16[704,256]{1,0:T(8,128)(2,1)} %bitcast.5, bf16[5632,256]{1,0:T(8,128)(2,1)} %w_down.1, bf16[32,2048]{1,0:T(8,128)(2,1)} %stream.1, f32[1,2048]{1,0:T(1,128)} %bitcast.7, bf16[2048,4096]{1,0:T(8,128)(2,1)} %vocab.1, ...), custom_call_target="tpu_custom_call" | custom-call | tf_op jit(solution)/shard_map/pallas_call | solution.py:622
  99.1 11.3 %shard_map.95 = (f32[512,4096]{1,0:T(8,128)}, f32[32,2048]{1,0:T(8,128)}, f32[1,32]{1,0:T(1,128)}) custom-call(bf16[512,1024]{1,0:T(8,128)(2,1)} %get-tuple-element.10.flipped, bf16[1024,4096]{1,0:T(8,128)(2,1)} %get-tuple-element.11.dscore, f32[32,2048]{1,0:T(8,128)} %get-tuple-element.12.grad_input, f32[8,256]{1,0:T(8,128)} %get-tuple-element.13.losses), custom_call_target="tpu_custom_call" | custom-call | tf_op jit(solution)/shard_map/pallas_call | solution.py:684
